TPU v7x, 512 devices: a whole 4x8x8 slice. The times are simulated.
512 devices in a mesh: fs: 128 (over z, y, core), tp: 4 (over x).
Axes of the slice: x: 4, y: 8, z: 8, core: 2. Of those that a mesh axis runs over, the one named last changes fastest.
Arguments:
- inputs: bfloat16 [73728, 2048], P('fs'), may hold values from -24 to 24
- query_cotangent: bfloat16 [73728, 1024], P('fs', 'tp'), may hold values from -0.017944336 to 0.017944336
- value_cotangent: bfloat16 [73728, 1024], P('fs', 'tp'), may hold values from -0.017944336 to 0.017944336
- weights_query: float32 [2048, 1024], P('fs', 'tp'), may hold values from -6 to 6
- weights_value: float32 [2048, 1024], P('fs', 'tp'), may hold values from -6 to 6
- basis_query: bfloat16 [1024, 32], P('tp'), may hold values from -0.75 to 0.75
- basis_value: bfloat16 [1024, 32], P('tp'), may hold values from -0.75 to 0.75
- first_query: float32 [2048, 512], P('fs', 'tp'), may hold values from -5.4 to 5.4, as said below
- second_query: float32 [2048, 512], P('fs', 'tp'), may hold values from 0.05 to 1
- first_value: float32 [2048, 512], P('fs', 'tp'), may hold values from -5.4 to 5.4, as said below
- second_value: float32 [2048, 512], P('fs', 'tp'), may hold values from 0.05 to 1
Outputs:
- step_query: float32 [2048, 1024], P('fs', 'tp')
- step_value: float32 [2048, 1024], P('fs', 'tp')
- new_query: float32 [2048, 1024], P('fs', 'tp')
- new_value: float32 [2048, 1024], P('fs', 'tp')
- copy_query: bfloat16 [2048, 1024], P(None, 'tp')
- copy_value: bfloat16 [2048, 1024], P(None, 'tp')
- moment_query: float32 [2048, 512], P('fs', 'tp')
- square_query: float32 [2048, 512], P('fs', 'tp')
- moment_value: float32 [2048, 512], P('fs', 'tp')
- square_value: float32 [2048, 512], P('fs', 'tp')
Inputs may be any that keep to these rules, and one draw needn't show every extreme that they name: `first_query`: first moments, with a spread of scale from row to row. `first_value`: first moments, with a spread of scale from row to row.
All inputs are finite; a program needn't handle non-finite values.
Results may differ from a plain program's by a relative error of at most 0.003.
Values may be sent and summed in bfloat16 or wider, within the bound.
A program may use at most 64 MiB of HBM per device.

v0:
```python
import jax
import jax.numpy as jnp
from jax import lax
from jax.sharding import Mesh
from jax.sharding import PartitionSpec as P

D = 2048
HEADS = 16
HEAD = 64
RK = 32
FS = ("fs_0", "fs_1", "fs_2")
FS_TP = ("fs_0", "fs_1", "fs_2", "tp")


def reduced_to_own(parts, axes, order):
    dims = [lax.axis_size(a) for a in axes]
    parts = parts.reshape(*dims, *parts.shape[1:])
    parts = parts.transpose(*order, *range(len(axes), parts.ndim))
    parts = parts.reshape(-1, *parts.shape[len(axes) :])
    for k in order:
        parts = lax.psum_scatter(parts, axes[k], scatter_dimension=0, tiled=True)
    return parts[0]


def in_blocks(value, dim, size):
    dims = value.shape
    parts = value.reshape(*dims[:dim], size, dims[dim] // size, *dims[dim + 1 :])
    return jnp.moveaxis(parts, dim, 0)


def scatter_axes(value, axes, order, dim):
    size = lax.axis_size(axes)
    return reduced_to_own(in_blocks(value, dim, size), axes, order)


def one_axis_at_a_time(value, axes):
    for axis in axes:
        value = lax.psum(value, axis)
    return value


def in_one_piece(arrays, axis, dim, along):
    widths = [a.shape[along] for a in arrays]
    both = jnp.concatenate(arrays, axis=along)
    filled = lax.all_gather(both, axis, axis=dim, tiled=True)
    return tuple(jnp.split(filled, [sum(widths[:k]) for k in range(1, len(widths))], axis=along))


def from_space(direction, factor, heads_here):
    count = direction.shape[0]
    split = direction.reshape(count, heads_here, RK)
    out = jnp.einsum("nhr,hdr->nhd", split, factor, precision=lax.Precision.HIGHEST)
    return out.reshape(count, heads_here * HEAD)


def moments(reduced, first, second):
    moment = 0.9 * first + 0.1 * reduced
    square = 0.95 * second + 0.05 * reduced * reduced
    direction = moment / (jnp.sqrt(square) + 1e-08)
    return (moment, square, direction)


def per_device(
    inputs,
    query_cotangent,
    value_cotangent,
    weights_query,
    weights_value,
    basis_query,
    basis_value,
    first_query,
    second_query,
    first_value,
    second_value,
):
    own_cols = weights_query.shape[1]
    heads_here = own_cols // HEAD
    space_cols = heads_here * RK
    factor_q = basis_query.reshape(heads_here, HEAD, RK).astype(jnp.float32)
    factor_v = basis_value.reshape(heads_here, HEAD, RK).astype(jnp.float32)
    contract = (((0,), (0,)), ((), ()))
    tok_count = query_cotangent.shape[0]
    bf_q = basis_query.reshape(heads_here, HEAD, RK)
    bf_v = basis_value.reshape(heads_here, HEAD, RK)
    small_q = jnp.einsum(
        "thd,hdr->thr",
        query_cotangent.reshape(tok_count, heads_here, HEAD),
        bf_q,
        preferred_element_type=jnp.float32,
    )
    small_v = jnp.einsum(
        "thd,hdr->thr",
        value_cotangent.reshape(tok_count, heads_here, HEAD),
        bf_v,
        preferred_element_type=jnp.float32,
    )
    small_both = jnp.concatenate(
        (small_q.reshape(tok_count, space_cols), small_v.reshape(tok_count, space_cols)), axis=1
    )
    upper_part = small_both.astype(jnp.bfloat16)
    lower_part = (small_both - upper_part.astype(jnp.float32)).astype(jnp.bfloat16)
    high = lax.dot_general(inputs, upper_part, contract, preferred_element_type=jnp.float32)
    reduced = scatter_axes(
        high + lax.dot_general(inputs, lower_part, contract, preferred_element_type=jnp.float32),
        FS,
        (2, 0, 1),
        0,
    )
    reduced_q = reduced[:, :space_cols]
    reduced_v = reduced[:, space_cols:]
    moment_q, square_q, direction_q = moments(reduced_q, first_query, second_query)
    moment_v, square_v, direction_v = moments(reduced_v, first_value, second_value)
    total_q, total_v = (
        one_axis_at_a_time(jnp.sum(direction_q * direction_q), FS_TP),
        one_axis_at_a_time(jnp.sum(direction_v * direction_v), FS_TP),
    )
    entries = D * HEADS * RK
    scale_q = 1.0 / jnp.sqrt(total_q / entries + 0.25)
    scale_v = 1.0 / jnp.sqrt(total_v / entries + 0.25)
    step_q = scale_q * from_space(direction_q, factor_q, heads_here)
    step_v = scale_v * from_space(direction_v, factor_v, heads_here)
    fresh_q = weights_query - 0.1 * step_q
    fresh_v = weights_value - 0.1 * step_v
    copy_q, copy_v = in_one_piece(
        (fresh_q.astype(jnp.bfloat16), fresh_v.astype(jnp.bfloat16)), FS, 0, 1
    )
    return (
        step_q,
        step_v,
        fresh_q,
        fresh_v,
        copy_q,
        copy_v,
        moment_q,
        square_q,
        moment_v,
        square_v,
    )


def solution(mesh):
    torus = Mesh(mesh.devices.reshape(8, 8, 2, mesh.shape["tp"]), ("fs_0", "fs_1", "fs_2", "tp"))
    return jax.shard_map(
        per_device,
        mesh=torus,
        in_specs=(
            P(FS, None),
            P(FS, "tp"),
            P(FS, "tp"),
            P(FS, "tp"),
            P(FS, "tp"),
            P("tp", None),
            P("tp", None),
            P(FS, "tp"),
            P(FS, "tp"),
            P(FS, "tp"),
            P(FS, "tp"),
        ),
        out_specs=(
            P(FS, "tp"),
            P(FS, "tp"),
            P(FS, "tp"),
            P(FS, "tp"),
            P(None, "tp"),
            P(None, "tp"),
            P(FS, "tp"),
            P(FS, "tp"),
            P(FS, "tp"),
            P(FS, "tp"),
        ),
        check_vma=False,
    )
```

profile of v0, /device:TPU:1, one launch (start us, length us, event | category | flops | bytes accessed | tf_op | source)
XLA Modules:
  0.0 274.1 jit_solution(18366344088311440782)
XLA Ops:
  7.2 0.0 copy-start
  7.2 0.0 reduce-scatter.4.cloned.1.call-start
  7.2 1.0 reshape.55
  8.2 0.8 reshape.58
  9.0 1.2 copy.41
  10.2 1.2 copy.43
  11.3 0.2 fusion.12
  11.5 0.2 fusion.9
  11.7 0.0 copy-done
  11.7 1.0 fusion.4
  12.7 2.3 fusion
  15.1 2.9 %copy.45 = f32[2048,256]{1,0:T(8,128)} copy(f32[2048,256]{0,1:T(8,128)} %fusion) | data formatting | bytes 4194304 | tf_op jit(solution)/shard_map/add | solution.py:104
  18.0 3.1 %copy.46 = f32[2,8,8,16,256]{4,3,2,1,0:T(8,128)} copy(f32[2,8,8,16,256]{4,3,0,2,1:T(8,128)} %bitcast.28) | data formatting | bytes 4194304 | tf_op jit(solution)/shard_map/transpose | solution.py:18
  21.1 0.0 copy-start.3
  21.1 0.0 copy-start.4
  21.2 0.0 reduce-scatter.4.cloned.1.call-update
  21.2 0.0 reduce-scatter.6.cloned.1.call-start
  21.2 24.5 %reduce-scatter.4.cloned.1.call-done = f32[64,16,256]{2,1,0:T(8,128)} async-done(((f32[128,16,256]{2,1,0:T(8,128)}), f32[64,16,256]{2,1,0:T(8,128)}) %reduce-scatter.4.cloned.1.call-update) | async-done | bytes 1048592 | tf_op jit(solution)/shard_map/reduce_scatter | solution.py:21
  45.7 0.0 reduce-scatter.6.cloned.1.call-update
  45.7 0.0 reduce-scatter.8.cloned.1.call-start
  45.8 41.3 %reduce-scatter.6.cloned.1.call-done = f32[8,16,256]{2,1,0:T(8,128)} async-done(((f32[64,16,256]{2,1,0:T(8,128)}), f32[8,16,256]{2,1,0:T(8,128)}) %reduce-scatter.6.cloned.1.call-update) | async-done | bytes 131088 | tf_op jit(solution)/shard_map/reduce_scatter | solution.py:21
  87.0 0.0 reduce-scatter.8.cloned.1.call-update
  87.0 0.0 all-gather.2.cloned.1.call-start
  87.1 39.1 %reduce-scatter.8.cloned.1.call-done = f32[1,16,256]{2,1,0:T(8,128)} async-done(((f32[8,16,256]{2,1,0:T(8,128)}), f32[1,16,256]{2,1,0:T(8,128)}) %reduce-scatter.8.cloned.1.call-update) | async-done | bytes 16400 | tf_op jit(solution)/shard_map/reduce_scatter | solution.py:21
  126.2 0.0 copy-done.5
  126.2 0.0 copy-done.6
  126.2 0.0 copy-done.7
  126.2 0.0 copy-done.8
  126.2 1.9 multiply_reduce_fusion
  128.1 15.0 %all-reduce.1 = (f32[]{:T(128)}, f32[]{:T(128)}) all-reduce(f32[]{:T(128)} %get-tuple-element.32, f32[]{:T(128)} %get-tuple-element.22), channel_id=1, replica_groups=mesh['fs_0'=8,'fs_1'=8,'fs_2'=2,'tp'=4] {'fs_0'}, use_global_device_ids=true, to_apply=%region_4.0 | all-reduce | flops 2 | bytes 16 | tf_op jit(solution)/shard_map/psum | solution.py:38
  143.1 12.8 %all-reduce = (f32[]{:T(128)}, f32[]{:T(128)}) all-reduce(f32[]{:T(128)} %get-tuple-element.12, f32[]{:T(128)} %get-tuple-element.13), channel_id=1, replica_groups=mesh['fs_0'=8,'fs_1'=8,'fs_2'=2,'tp'=4] {'fs_1'}, use_global_device_ids=true, to_apply=%region_5.0 | all-reduce | flops 2 | bytes 16 | tf_op jit(solution)/shard_map/psum | solution.py:38
  155.9 16.1 %all-reduce.3 = (f32[]{:T(128)}, f32[]{:T(128)}) all-reduce(f32[]{:T(128)} %get-tuple-element.10, f32[]{:T(128)} %get-tuple-element.11), channel_id=1, replica_groups=mesh['fs_0'=8,'fs_1'=8,'fs_2'=2,'tp'=4] {'fs_2'}, use_global_device_ids=true, to_apply=%region_6.0 | all-reduce | flops 2 | bytes 16 | tf_op jit(solution)/shard_map/psum | solution.py:38
  172.0 9.0 %all-reduce.2 = (f32[]{:T(128)}, f32[]{:T(128)}) all-reduce(f32[]{:T(128)} %get-tuple-element.16, f32[]{:T(128)} %get-tuple-element.17), channel_id=1, replica_groups=mesh['fs_0'=8,'fs_1'=8,'fs_2'=2,'tp'=4] {'tp'}, use_global_device_ids=true, to_apply=%region_7.0 | all-reduce | flops 2 | bytes 16 | tf_op jit(solution)/shard_map/psum | solution.py:38
  182.4 0.1 reshape.63
  182.4 0.1 fusion.1
  182.6 0.1 mul.85
  182.7 0.1 reshape.62
  182.8 0.1 fusion.2
  183.0 0.1 mul.75
  183.1 0.0 copy-done.3
  183.1 0.0 copy-done.4
  183.1 0.6 fusion.18
  183.7 0.6 pad_maximum_fusion.1
  184.3 0.0 all-gather.2.cloned.1.call-update
  184.3 80.3 %all-gather.2.cloned.1.call-done = bf16[2048,512]{1,0:T(8,128)(2,1)} async-done(((bf16[16,512]{1,0:T(8,128)(2,1)}), bf16[2048,512]{1,0:T(8,128)(2,1)}) %all-gather.2.cloned.1.call-update) | async-done | bytes 2097168 | tf_op jit(solution)/shard_map/all_gather | solution.py:45
  264.6 3.0 %fusion.22 = (bf16[2048,256]{1,0:T(8,128)(2,1)}, bf16[2048,256]{1,0:T(8,128)(2,1)}) fusion(bf16[2048,512]{1,0:T(8,128)(2,1)} %all-gather.2.cloned.1.call-done), kind=kLoop, calls=%fused_computation.35 | loop fusion | bytes 4194304 | tf_op jit(solution)/shard_map/split | solution.py:46
  267.6 0.0 copy-done.1
  267.6 0.0 copy-done.2
  (8 shorter events, 0.0 us)
Async XLA Ops:
  7.2 4.6 %copy-start = (bf16[576,2048]{1,0:T(8,128)(2,1)S(1)}, bf16[576,2048]{1,0:T(8,128)(2,1)}, u32[]{:S(2)}) copy-start(bf16[576,2048]{1,0:T(8,128)(2,1)} %param.11) | copy-start | bytes 7077892
  7.2 38.5 %reduce-scatter.4.cloned.1.call-start = ((), (), s32[]{:S(2)}) async-start(), calls=%async_computation.3 | async-start | bytes 3145728 | tf_op jit(solution)/shard_map/reduce_scatter | solution.py:21
  21.1 105.0 %copy-start.5 = (f32[16,128]{1,0:T(8,128)S(1)}, f32[16,128]{1,0:T(8,128)}, u32[]{:S(2)}) copy-start(f32[16,128]{1,0:T(8,128)} %param.21) | copy-start | bytes 24580
  21.1 105.0 %copy-start.6 = (f32[16,128]{1,0:T(8,128)S(1)}, f32[16,128]{1,0:T(8,128)}, u32[]{:S(2)}) copy-start(f32[16,128]{1,0:T(8,128)} %param.20) | copy-start | bytes 24580
  21.1 105.0 %copy-start.7 = (f32[16,128]{1,0:T(8,128)S(1)}, f32[16,128]{1,0:T(8,128)}, u32[]{:S(2)}) copy-start(f32[16,128]{1,0:T(8,128)} %param.19) | copy-start | bytes 24580
  21.1 105.0 %copy-start.8 = (f32[16,128]{1,0:T(8,128)S(1)}, f32[16,128]{1,0:T(8,128)}, u32[]{:S(2)}) copy-start(f32[16,128]{1,0:T(8,128)} %param.18) | copy-start | bytes 24580
  21.1 161.9 %copy-start.3 = (f32[16,256]{1,0:T(8,128)S(1)}, f32[16,256]{1,0:T(8,128)}, u32[]{:S(2)}) copy-start(f32[16,256]{1,0:T(8,128)} %param.14) | copy-start | bytes 49156
  21.1 161.9 %copy-start.4 = (f32[16,256]{1,0:T(8,128)S(1)}, f32[16,256]{1,0:T(8,128)}, u32[]{:S(2)}) copy-start(f32[16,256]{1,0:T(8,128)} %param.15) | copy-start | bytes 49156
  21.2 65.8 %reduce-scatter.6.cloned.1.call-start = ((), (), s32[]{:S(2)}) async-start(), calls=%async_computation.4 | async-start | bytes 1179648 | tf_op jit(solution)/shard_map/reduce_scatter | solution.py:21
  45.7 80.5 %reduce-scatter.8.cloned.1.call-start = ((), (), s32[]{:S(2)}) async-start(), calls=%async_computation.5 | async-start | bytes 147456 | tf_op jit(solution)/shard_map/reduce_scatter | solution.py:21
  87.0 177.6 %all-gather.2.cloned.1.call-start = ((), (), s32[]{:S(2)}) async-start(), calls=%async_computation.6 | async-start | bytes 2113536 | tf_op jit(solution)/shard_map/all_gather | solution.py:45
  182.7 84.9 %copy-start.1 = (f32[16,256]{1,0:T(8,128)}, f32[16,256]{1,0:T(8,128)S(1)}, u32[]{:S(2)}) copy-start(f32[16,256]{1,0:T(8,128)S(1)} %mul.85) | copy-start | bytes 49156
  183.1 84.5 %copy-start.2 = (f32[16,256]{1,0:T(8,128)}, f32[16,256]{1,0:T(8,128)S(1)}, u32[]{:S(2)}) copy-start(f32[16,256]{1,0:T(8,128)S(1)} %mul.75) | copy-start | bytes 49156
Sparse Core Ops, SparseCore 0:
  21.3 24.3 reduce-scatter.3
  48.5 38.4 reduce-scatter.5
  89.8 36.3 reduce-scatter.7
  184.4 80.1 all-gather.1
where the time goes:
time: 275 us; the launch traced here: 274 us
  waiting for transfers between devices  185 us (67%)
  blocking collectives  52.9 us (19%)
  between operations  15.3 us (6%)
  local copies, waits for them, and re-layouts  13.6 us (5%)
  matrix products  3.98 us (1%)
  other arithmetic  3.17 us (1%)
    reduce_scatter x3, waiting for transfers between devices, reduced_to_own(): parts = lax.psum_scatter(parts, axes[k], scatter_dimension=0, tiled=True)  105 us
    all_gather x1, waiting for transfers between devices, in_one_piece(): filled = lax.all_gather(both, axis, axis=dim, tiled=True)  80.3 us
    psum x4, blocking collectives, one_axis_at_a_time(): value = lax.psum(value, axis)  52.9 us
  transfers between devices with their start and end apart: 4, of which 4 were waited for; matrix products, arithmetic and copies ran while one was open for 0% of the time, Pallas kernels for 0%

commit v1 on v0

--- a/solution.py
+++ b/solution.py
@@ -35,7 +35,7 @@
 
 def one_axis_at_a_time(value, axes):
     for axis in axes:
-        value = lax.psum(value, axis)
+        value = jnp.sum(lax.all_gather(value, axis), 0)
     return value
 
 

time: 275 us -> 292 us (1.062)
  local copies, waits for them, and re-layouts: 13.6 us -> 29.8 us
  other arithmetic: 3.17 us -> 7.98 us
    psum x4 -> x0, blocking collectives: 52.9 us -> none  [one_axis_at_a_time(): value = lax.psum(value, axis)]
    unnamed x0 -> x4, blocking collectives: none -> 50.3 us
    unnamed x20 -> x40, local copies, waits for them, and re-layouts: 2.37 us -> 18.7 us
    reduce_sum x0 -> x8, other arithmetic: none -> 4.81 us  [one_axis_at_a_time(): value = jnp.sum(lax.all_gather(value, axis), 0)]
where the time goes in v1:
time: 292 us; the launch traced here: 291 us
  waiting for transfers between devices  184 us (63%)
  blocking collectives  50.3 us (17%)
  local copies, waits for them, and re-layouts  29.8 us (10%)
  between operations  15.3 us (5%)
  other arithmetic  7.98 us (3%)
  matrix products  3.97 us (1%)
    reduce_scatter x3, waiting for transfers between devices, reduced_to_own(): parts = lax.psum_scatter(parts, axes[k], scatter_dimension=0, tiled=True)  104 us
    all_gather x1, waiting for transfers between devices, in_one_piece(): filled = lax.all_gather(both, axis, axis=dim, tiled=True)  80.3 us
    unnamed x4, blocking collectives  50.3 us
    unnamed x40, local copies, waits for them, and re-layouts  18.7 us
  transfers between devices with their start and end apart: 4, of which 4 were waited for; matrix products, arithmetic and copies ran while one was open for 0% of the time, Pallas kernels for 0%

profile of v1, /device:TPU:1, one launch (start us, length us, event | category | flops | bytes accessed | tf_op | source)
XLA Modules:
  0.0 291.4 jit_solution(12437111014980550797)
XLA Ops:
  7.2 1.0 reshape.55
  8.2 0.8 reshape.58
  9.0 1.2 copy.41
  10.2 1.2 copy.43
  11.3 0.2 fusion.12
  11.5 0.2 fusion.9
  11.7 1.0 fusion.4
  12.7 2.3 fusion
  15.0 2.9 %copy.45 = f32[2048,256]{1,0:T(8,128)} copy(f32[2048,256]{0,1:T(8,128)} %fusion) | data formatting | bytes 4194304 | tf_op jit(solution)/shard_map/add | solution.py:104
  18.0 3.1 %copy.46 = f32[2,8,8,16,256]{4,3,2,1,0:T(8,128)} copy(f32[2,8,8,16,256]{4,3,0,2,1:T(8,128)} %bitcast.40) | data formatting | bytes 4194304 | tf_op jit(solution)/shard_map/transpose | solution.py:18
  21.2 24.5 %reduce-scatter.4.cloned.1.call-done = f32[64,16,256]{2,1,0:T(8,128)} async-done(((f32[128,16,256]{2,1,0:T(8,128)}), f32[64,16,256]{2,1,0:T(8,128)}) %reduce-scatter.4.cloned.1.call-update) | async-done | bytes 1048592 | tf_op jit(solution)/shard_map/reduce_scatter | solution.py:21
  45.7 41.3 %reduce-scatter.6.cloned.1.call-done = f32[8,16,256]{2,1,0:T(8,128)} async-done(((f32[64,16,256]{2,1,0:T(8,128)}), f32[8,16,256]{2,1,0:T(8,128)}) %reduce-scatter.6.cloned.1.call-update) | async-done | bytes 131088 | tf_op jit(solution)/shard_map/reduce_scatter | solution.py:21
  87.1 1.3 dynamic-slice
  88.4 37.8 %reduce-scatter.8.cloned.1.call-done = f32[1,16,256]{2,1,0:T(8,128)} async-done(((f32[8,16,256]{2,1,0:T(8,128)}), f32[1,16,256]{2,1,0:T(8,128)}) %reduce-scatter.8.cloned.1.call-update) | async-done | bytes 16400 | tf_op jit(solution)/shard_map/reduce_scatter | solution.py:21
  126.2 1.9 multiply_reduce_fusion
  128.1 1.4 dynamic-update-slice.4
  129.5 1.4 dynamic-update-slice
  130.9 1.3 dynamic-slice.1
  132.2 14.4 %all-reduce.9 = (f32[8]{0:T(128)S(1)}, f32[8]{0:T(128)S(1)}) all-reduce(f32[8]{0:T(128)S(1)} %dynamic-update-slice, f32[8]{0:T(128)S(1)} %dynamic-update-slice.4), channel_id=1, replica_groups=mesh['fs_0'=8,'fs_1'=8,'fs_2'=2,'tp'=4] {'fs_0'}, use_global_device_ids=true, to_apply=%add | all-reduce | flops 16 | bytes 128
  146.5 0.6 reduce_sum.96
  147.1 0.6 reduce_sum.91
  147.7 1.4 dynamic-update-slice.5
  149.1 1.4 dynamic-update-slice.1
  150.5 1.3 dynamic-slice.2
  151.8 11.9 %all-reduce.8 = (f32[8]{0:T(128)S(1)}, f32[8]{0:T(128)S(1)}) all-reduce(f32[8]{0:T(128)S(1)} %dynamic-update-slice.1, f32[8]{0:T(128)S(1)} %dynamic-update-slice.5), channel_id=1, replica_groups=mesh['fs_0'=8,'fs_1'=8,'fs_2'=2,'tp'=4] {'fs_1'}, use_global_device_ids=true, to_apply=%add.1 | all-reduce | flops 16 | bytes 128
  163.7 0.6 reduce_sum.97
  164.3 0.6 reduce_sum.92
  164.9 1.4 dynamic-update-slice.6
  166.3 1.4 dynamic-update-slice.2
  167.7 1.3 dynamic-slice.3
  169.0 15.6 %all-reduce.11 = (f32[2]{0:T(128)S(1)}, f32[2]{0:T(128)S(1)}) all-reduce(f32[2]{0:T(128)S(1)} %dynamic-update-slice.2, f32[2]{0:T(128)S(1)} %dynamic-update-slice.6), channel_id=1, replica_groups=mesh['fs_0'=8,'fs_1'=8,'fs_2'=2,'tp'=4] {'fs_2'}, use_global_device_ids=true, to_apply=%add.2 | all-reduce | flops 4 | bytes 32
  184.7 0.6 reduce_sum.98
  185.3 0.6 reduce_sum.93
  185.9 1.4 dynamic-update-slice.7
  187.3 1.4 dynamic-update-slice.3
  188.7 8.4 %all-reduce.10 = (f32[4]{0:T(128)S(1)}, f32[4]{0:T(128)S(1)}) all-reduce(f32[4]{0:T(128)S(1)} %dynamic-update-slice.3, f32[4]{0:T(128)S(1)} %dynamic-update-slice.7), channel_id=1, replica_groups=mesh['fs_0'=8,'fs_1'=8,'fs_2'=2,'tp'=4] {'tp'}, use_global_device_ids=true, to_apply=%add.3 | all-reduce | flops 8 | bytes 64
  197.1 0.6 reduce_sum.99
  198.4 0.6 reduce_sum.94
  199.7 0.1 reshape.63
  199.7 0.1 fusion.1
  199.9 0.1 mul.85
  200.0 0.1 reshape.62
  200.1 0.1 fusion.2
  200.3 0.1 mul.75
  200.4 0.6 fusion.18
  201.0 0.6 pad_maximum_fusion.1
  201.6 80.3 %all-gather.2.cloned.1.call-done = bf16[2048,512]{1,0:T(8,128)(2,1)} async-done(((bf16[16,512]{1,0:T(8,128)(2,1)}), bf16[2048,512]{1,0:T(8,128)(2,1)}) %all-gather.2.cloned.1.call-update) | async-done | bytes 2097168 | tf_op jit(solution)/shard_map/all_gather | solution.py:45
  281.9 3.0 %fusion.22 = (bf16[2048,256]{1,0:T(8,128)(2,1)}, bf16[2048,256]{1,0:T(8,128)(2,1)}) fusion(bf16[2048,512]{1,0:T(8,128)(2,1)} %all-gather.2.cloned.1.call-done), kind=kLoop, calls=%fused_computation.35 | loop fusion | bytes 4194304 | tf_op jit(solution)/shard_map/split | solution.py:46
  (36 shorter events, 0.3 us)
Async XLA Ops:
  7.2 4.6 %copy-start = (bf16[576,2048]{1,0:T(8,128)(2,1)S(1)}, bf16[576,2048]{1,0:T(8,128)(2,1)}, u32[]{:S(2)}) copy-start(bf16[576,2048]{1,0:T(8,128)(2,1)} %param.11) | copy-start | bytes 7077892
  7.2 38.5 %reduce-scatter.4.cloned.1.call-start = ((), (), s32[]{:S(2)}) async-start(), calls=%async_computation.3 | async-start | bytes 3145728 | tf_op jit(solution)/shard_map/reduce_scatter | solution.py:21
  21.1 105.0 %copy-start.5 = (f32[16,128]{1,0:T(8,128)S(1)}, f32[16,128]{1,0:T(8,128)}, u32[]{:S(2)}) copy-start(f32[16,128]{1,0:T(8,128)} %param.21) | copy-start | bytes 24580
  21.1 105.0 %copy-start.6 = (f32[16,128]{1,0:T(8,128)S(1)}, f32[16,128]{1,0:T(8,128)}, u32[]{:S(2)}) copy-start(f32[16,128]{1,0:T(8,128)} %param.20) | copy-start | bytes 24580
  21.1 105.0 %copy-start.7 = (f32[16,128]{1,0:T(8,128)S(1)}, f32[16,128]{1,0:T(8,128)}, u32[]{:S(2)}) copy-start(f32[16,128]{1,0:T(8,128)} %param.19) | copy-start | bytes 24580
  21.1 105.0 %copy-start.8 = (f32[16,128]{1,0:T(8,128)S(1)}, f32[16,128]{1,0:T(8,128)}, u32[]{:S(2)}) copy-start(f32[16,128]{1,0:T(8,128)} %param.18) | copy-start | bytes 24580
  21.1 179.2 %copy-start.3 = (f32[16,256]{1,0:T(8,128)S(1)}, f32[16,256]{1,0:T(8,128)}, u32[]{:S(2)}) copy-start(f32[16,256]{1,0:T(8,128)} %param.14) | copy-start | bytes 49156
  21.1 179.2 %copy-start.4 = (f32[16,256]{1,0:T(8,128)S(1)}, f32[16,256]{1,0:T(8,128)}, u32[]{:S(2)}) copy-start(f32[16,256]{1,0:T(8,128)} %param.15) | copy-start | bytes 49156
  21.2 65.8 %reduce-scatter.6.cloned.1.call-start = ((), (), s32[]{:S(2)}) async-start(), calls=%async_computation.4 | async-start | bytes 1179648 | tf_op jit(solution)/shard_map/reduce_scatter | solution.py:21
  45.7 80.5 %reduce-scatter.8.cloned.1.call-start = ((), (), s32[]{:S(2)}) async-start(), calls=%async_computation.5 | async-start | bytes 147456 | tf_op jit(solution)/shard_map/reduce_scatter | solution.py:21
  87.0 194.9 %all-gather.2.cloned.1.call-start = ((), (), s32[]{:S(2)}) async-start(), calls=%async_computation.6 | async-start | bytes 2113536 | tf_op jit(solution)/shard_map/all_gather | solution.py:45
  200.0 84.9 %copy-start.1 = (f32[16,256]{1,0:T(8,128)}, f32[16,256]{1,0:T(8,128)S(1)}, u32[]{:S(2)}) copy-start(f32[16,256]{1,0:T(8,128)S(1)} %mul.85) | copy-start | bytes 49156
  200.4 84.5 %copy-start.2 = (f32[16,256]{1,0:T(8,128)}, f32[16,256]{1,0:T(8,128)S(1)}, u32[]{:S(2)}) copy-start(f32[16,256]{1,0:T(8,128)S(1)} %mul.75) | copy-start | bytes 49156
Sparse Core Ops, SparseCore 0:
  21.3 24.3 reduce-scatter.3
  48.5 38.4 reduce-scatter.5
  89.8 36.3 reduce-scatter.7
  201.7 80.1 all-gather.1
